TPU v7x, 256 devices: a 4x2x16 block of a 4x16x16 slice. The times are simulated.
256 devices in a mesh: grp: 2 (over y), sp: 32 (over z, core), tp: 4 (over x).
Axes of the slice: x: 4, y: 2, z: 16, core: 2. Of those that a mesh axis runs over, the one named last changes fastest.
The devices are a block of a 4x16x16 slice.
Arguments:
- gate_in: bfloat16 [32768, 1536], P(('grp', 'sp'), 'tp'), parts along dimension 0, may hold values from -6 to 6
- mult_in: bfloat16 [32768, 1536], P(('grp', 'sp'), 'tp'), parts along dimension 0, may hold values from -6 to 6
- value_in: bfloat16 [32768, 1536], P(('grp', 'sp'), 'tp'), parts along dimension 0, may hold values from -6 to 6
- doc_ids: int32 [32768], P(('grp', 'sp')), parts along dimension 0, may hold values from 0 to 15, never falling along the last dimension, each value on 1 to 1536 neighbouring positions
- conv_taps: bfloat16 [3, 1536], P(None, 'tp'), may hold values from -3 to 3
- out_proj: bfloat16 [1536, 2048], P('tp'), may hold values from -0.15625 to 0.15625
- resid: bfloat16 [32768, 2048], P(('grp', 'sp', 'tp')), parts along dimension 0, may hold values from -6 to 6
- norm1_gain: float32 [2048], replicated, may hold values from 0.1 to 1.9
- norm1_bias: float32 [2048], replicated, may hold values from -1.5 to 1.5
- expert_ids: int32 [32768, 2], P(('grp', 'sp', 'tp')), parts along dimension 0, may hold values from 0 to 31, all different within a row; in each aligned block of 128 rows (0 to 127, 128 to 255, ...) at most 10 rows name the same one
- expert_wts: float32 [32768, 2], P(('grp', 'sp', 'tp')), parts along dimension 0, may hold values from 0.1 to 1
- w_gate: bfloat16 [32, 2048, 3072], P('sp', None, 'tp'), may hold values from -0.125 to 0.125
- w_up: bfloat16 [32, 2048, 3072], P('sp', None, 'tp'), may hold values from -0.125 to 0.125
- w_down: bfloat16 [32, 3072, 2048], P('sp', 'tp'), may hold values from -0.21582031 to 0.21582031
- norm2_gain: float32 [2048], replicated, may hold values from 0.1 to 1.9
- norm2_bias: float32 [2048], replicated, may hold values from -1.5 to 1.5
Outputs:
- result: bfloat16 [32768, 2048], P(('grp', 'sp', 'tp')), parts along dimension 0
There are 2 independent parts, one for each index of `grp`. A program takes and returns all parts, laid end to end along the dimension named above; an argument that names none is the same for every part. Nothing has to cross between parts.
Inputs may be any that keep to these rules, and one draw needn't show every extreme that they name: `doc_ids`: never falling along the sequence; each document has 1 to 1536 positions and one has exactly 1536. `expert_ids`: each row names 2 different experts. Among the rows of one device no expert is named more than 10 times, and in some device's rows some expert is named exactly 10 times.
All inputs are finite; a program needn't handle non-finite values.
Results may differ from a plain program's by a relative error of at most 0.0095.
Values may be sent and summed in bfloat16 or wider, within the bound.
No kernel may reach another device: no remote copies, remote signals or barrier semaphores. Data moves between devices by JAX's collectives and lax.ppermute only.
A program may use at most 128 MiB of HBM per device.

v0:
```python
import jax
import jax.numpy as jnp
from jax import lax
from jax.sharding import Mesh
from jax.sharding import PartitionSpec as P

SP = ("sp_0", "sp_1")
GRP_SP = ("grp", "sp_0", "sp_1")
GRP_SP_TP = ("grp", "sp_0", "sp_1", "tp")


residual_scale = 2.0**0.5
norm_eps = 1e-05


def shifted_2(x, axis, by):
    length = lax.axis_size(axis)
    pairs = [(i, i + by) for i in range(length) if 0 <= i + by < length]
    return lax.ppermute(x, axis, pairs)


def split_up(x, dim, length):
    before, after = (x.shape[:dim], x.shape[dim + 1 :])
    return jnp.moveaxis(x.reshape(*before, length, -1, *after), dim, 0)


def summed_on_arrival(x, axis, dim):
    length = lax.axis_size(axis)
    tiles = lax.all_to_all(split_up(x, dim, length), axis, 0, 0, tiled=True)
    return jnp.sum(tiles.astype(jnp.float32), axis=0)


def joined_along(tiles, dim):
    lengths = list(tiles.shape[1:])
    lengths[dim] *= tiles.shape[0]
    return jnp.moveaxis(tiles, 0, dim).reshape(lengths)


def moved_by_axis(tiles, axes, sequence):
    lengths = [lax.axis_size(a) for a in axes]
    tiles = tiles.reshape(*lengths, *tiles.shape[1:])
    for k in sequence:
        tiles = lax.all_to_all(tiles, axes[k], split_axis=k, concat_axis=k, tiled=True)
    return tiles.reshape(-1, *tiles.shape[len(axes) :])


def two_step_exchange(x, groups, sequence, split_dim, concat_dim):
    length = lax.axis_size(groups[0]) * lax.axis_size(groups[1])
    tiles = split_up(x, split_dim, length)
    return joined_along(moved_by_axis(tiles, groups, sequence), concat_dim)


def layer_norm(pre, gain, bias):
    center = pre - jnp.mean(pre, axis=-1, keepdims=True)
    spread = jnp.mean(center * center, axis=-1, keepdims=True)
    return center * lax.rsqrt(spread + norm_eps) * gain + bias


def shards(
    gate_in,
    mult_in,
    value_in,
    doc_ids,
    conv_taps,
    out_proj,
    resid,
    norm1_gain,
    norm1_bias,
    expert_ids,
    expert_wts,
    w_gate,
    w_up,
    w_down,
    norm2_gain,
    norm2_bias,
):
    tap_weights = conv_taps.astype(jnp.float32)
    kernel_width = tap_weights.shape[0]
    product = mult_in.astype(jnp.float32) * value_in.astype(jnp.float32)
    doc_numbers = doc_ids.astype(jnp.float32)
    row_count = product.shape[0]
    prev_rows, prev_docs = shifted_2(
        (product[row_count - kernel_width + 1 :], doc_numbers[row_count - kernel_width + 1 :]),
        SP,
        1,
    )
    ext_rows = jnp.concatenate([prev_rows, product], axis=0)
    ext_docs = jnp.concatenate([prev_docs, doc_numbers], axis=0)
    filtered = jnp.zeros_like(product)
    for tap_index in range(kernel_width):
        shifted = ext_rows[tap_index : tap_index + row_count]
        same_doc = (ext_docs[tap_index : tap_index + row_count] == doc_numbers)[:, None]
        filtered = filtered + tap_weights[tap_index] * jnp.where(same_doc, shifted, 0.0)
    mixed_heads = (gate_in.astype(jnp.float32) * filtered).astype(jnp.bfloat16)
    tok_rows = lax.all_to_all(mixed_heads, "tp", split_axis=0, concat_axis=1, tiled=True)
    model_width = out_proj.shape[1]
    mixed = jnp.dot(
        tok_rows,
        lax.all_gather(out_proj, "tp", axis=0, tiled=True),
        preferred_element_type=jnp.float32,
    )
    hidden_one = layer_norm(
        residual_scale * resid.astype(jnp.float32) + mixed, norm1_gain, norm1_bias
    ).astype(jnp.bfloat16)
    tok_count = expert_ids.shape[0]
    top_count = expert_ids.shape[1]
    experts = lax.axis_size(SP)
    capacity = 5 * tok_count * top_count // (4 * experts)
    flat_ids = expert_ids.reshape(-1)
    one_hot = (flat_ids[:, None] == jnp.arange(experts, dtype=jnp.int32)[None, :]).astype(jnp.int32)
    earlier = jnp.cumsum(one_hot, axis=0) - one_hot
    slot_index = jnp.sum(earlier * one_hot, axis=1)
    dest_slot = (flat_ids * capacity + slot_index).reshape(tok_count, top_count)
    slot_ids = jnp.arange(experts * capacity, dtype=jnp.int32)
    selector = jnp.any(slot_ids[:, None, None] == dest_slot[None, :, :], axis=2).astype(
        jnp.bfloat16
    )
    packed = jnp.dot(selector, hidden_one, preferred_element_type=jnp.float32).astype(jnp.bfloat16)
    packed = packed.reshape(experts, capacity, model_width)
    whole = lax.all_gather(
        two_step_exchange(packed, ("sp_0", "sp_1"), (1, 0), 0, 0), "tp", axis=0, tiled=True
    )
    shape_in = whole.shape
    rows_in = whole.reshape(-1, shape_in[-1])
    gate_act = jnp.dot(rows_in, w_gate[0], preferred_element_type=jnp.float32)
    up_act = jnp.dot(rows_in, w_up[0], preferred_element_type=jnp.float32)
    hid = (jax.nn.silu(gate_act) * up_act).astype(jnp.bfloat16)
    summed = summed_on_arrival(
        jnp.dot(hid, w_down[0], preferred_element_type=jnp.float32)
        .astype(jnp.bfloat16)
        .reshape(shape_in),
        "tp",
        0,
    )
    expert_out = two_step_exchange(summed.astype(jnp.bfloat16), ("sp_0", "sp_1"), (1, 0), 0, 0)
    expert_flat = expert_out.reshape(experts * capacity, model_width)
    picked = jnp.take(expert_flat, dest_slot, axis=0)
    moe = jnp.sum(expert_wts[:, :, None] * picked.astype(jnp.float32), axis=1)
    return layer_norm(
        residual_scale * hidden_one.astype(jnp.float32) + moe, norm2_gain, norm2_bias
    ).astype(jnp.bfloat16)


def solution(mesh):
    torus = Mesh(
        mesh.devices.reshape(mesh.shape["grp"], 16, 2, mesh.shape["tp"]),
        ("grp", "sp_0", "sp_1", "tp"),
    )
    in_specs = (
        P(GRP_SP, "tp"),
        P(GRP_SP, "tp"),
        P(GRP_SP, "tp"),
        P(GRP_SP),
        P(None, "tp"),
        P("tp", None),
        P(GRP_SP_TP, None),
        P(),
        P(),
        P(GRP_SP_TP, None),
        P(GRP_SP_TP, None),
        P(SP, None, "tp"),
        P(SP, None, "tp"),
        P(SP, "tp", None),
        P(),
        P(),
    )
    out_specs = P(GRP_SP_TP, None)
    return jax.shard_map(
        shards, mesh=torus, in_specs=in_specs, out_specs=out_specs, check_vma=False
    )
```

profile of v0, /device:TPU:40, one launch (start us, length us, event | category | flops | bytes accessed | tf_op | source)
XLA Modules:
  0.0 478.0 jit_solution(11443134529266028846)
XLA Ops:
  8.3 1.8 collective-permute-start
  12.2 4.9 %collective-permute-start.1 = (f32[2,384]{1,0:T(2,128)S(1)}, f32[2,384]{1,0:T(2,128)S(1)}, u32[]{:S(2)}, u32[]{:S(2)}) collective-permute-start(f32[2,384]{1,0:T(2,128)S(1)} %slice.47), channel_id=1, source_target_pairs={{0,4},{4,8},{8,12},{12,16},{16,20},{20,24},{24,28},{28,32},{32,36}... | collective-permute-start | bytes 9224 | tf_op jit(solution)/shard_map/ppermute | solution.py:19
  18.9 3.1 fusion.11
  22.0 4.6 all-to-all-start
  28.4 6.4 %all-to-all-done = bf16[4,128,384]{2,1,0:T(8,128)(2,1)S(1)} async-done(((bf16[4,128,384]{2,1,0:T(8,128)(2,1)}), bf16[4,128,384]{2,1,0:T(8,128)(2,1)S(1)}, u32[]{:S(2)}, u32[]{:S(2)}) %all-to-all-start) | async-done | bytes 393248 | tf_op jit(solution)/shard_map/all_to_all | solution.py:95
  36.8 57.4 %all-gather.3.cloned.1.call-done = bf16[1536,2048]{1,0:T(8,128)(2,1)} async-done(((bf16[384,2048]{1,0:T(8,128)(2,1)}), bf16[1536,2048]{1,0:T(8,128)(2,1)}) %all-gather.3.cloned.1.call-update) | async-done | bytes 6291472 | tf_op jit(solution)/shard_map/all_gather | solution.py:99
  94.2 4.0 fusion.20
  99.1 1.7 convolution_convert_fusion.1
  100.8 3.3 reshape_reshape_reshape.6
  104.1 2.3 copy.84
  106.5 4.8 %all_to_all.44 = bf16[16,2,1,10,2048]{4,0,3,2,1:T(8,128)(2,1)S(1)} all-to-all(bf16[16,2,1,10,2048]{4,0,3,2,1:T(8,128)(2,1)S(1)} %copy.84), channel_id=1, replica_groups=mesh['grp'=2,'sp_0'=16,'sp_1'=2,'tp'=4] {'sp_1'}, dimensions={1} | all-to-all | bytes 2621440 | tf_op jit(solution)/shard_map/all_to_all | solution.py:43
  112.6 77.5 %all_to_all.45 = bf16[16,2,1,10,2048]{4,1,3,2,0:T(2,128)(2,1)S(1)} all-to-all(bf16[16,2,1,10,2048]{4,1,3,2,0:T(2,128)(2,1)S(1)} %copy.85), channel_id=1, replica_groups=mesh['grp'=2,'sp_0'=16,'sp_1'=2,'tp'=4] {'sp_0'}, dimensions={0} | all-to-all | bytes 2621440 | tf_op jit(solution)/shard_map/all_to_all | solution.py:43
  190.1 2.2 copy.86
  192.3 4.1 reshape_reshape.9
  196.4 56.1 %all-gather.5.cloned.1.call-done = bf16[128,10,2048]{2,0,1:T(8,128)(2,1)} async-done(((bf16[32,10,2048]{2,0,1:T(8,128)(2,1)}), bf16[128,10,2048]{2,0,1:T(8,128)(2,1)}) %all-gather.5.cloned.1.call-update) | async-done | bytes 5242896 | tf_op jit(solution)/shard_map/all_gather | solution.py:120
  252.6 9.0 %copy.87 = bf16[128,10,2048]{2,1,0:T(8,128)(2,1)} copy(bf16[128,10,2048]{2,0,1:T(8,128)(2,1)} %all-gather.5.cloned.1.call-done) | data formatting | bytes 10485760 | tf_op jit(solution)/shard_map/all_gather | solution.py:120
  261.6 9.8 %reshape.70 = bf16[1280,2048]{1,0:T(8,128)(2,1)} reshape(bf16[128,10,2048]{2,1,0:T(8,128)(2,1)} %copy.87) | data formatting | bytes 10485760 | tf_op jit(solution)/shard_map/reshape | solution.py:124
  271.4 7.2 %fusion.3 = f32[1280,768]{1,0:T(8,128)S(1)} fusion(bf16[1280,2048]{1,0:T(8,128)(2,1)} %reshape.70, bf16[1,2048,768]{2,1,0:T(8,128)(2,1)} %param.27), kind=kOutput, calls=%fused_computation.6 | convolution fusion | flops 4026531840 | bytes 12320768 | tf_op jit(solution)/shard_map/dot_general | solution.py:125
  278.7 4.8 %fusion = bf16[1280,768]{1,0:T(8,128)(2,1)S(1)} fusion(bf16[1280,2048]{1,0:T(8,128)(2,1)S(1)} %copy-done.4, f32[1280,768]{1,0:T(8,128)S(1)} %fusion.3, bf16[1,2048,768]{2,1,0:T(8,128)(2,1)S(1)} %copy-done.19), kind=kOutput, calls=%fused_computation.3 | convolution fusion | flops 4032430080 | bytes 14286848 | tf_op jit(solution)/shard_map/dot_general | solution.py:126
  283.5 6.3 %convolution_convert_fusion = bf16[1280,2048]{1,0:T(8,128)(2,1)} fusion(bf16[1280,768]{1,0:T(8,128)(2,1)S(1)} %fusion, bf16[1,768,2048]{2,1,0:T(8,128)(2,1)S(1)} %copy-done), kind=kOutput, calls=%fused_computation.1 | convolution fusion | flops 4029153280 | bytes 10354688 | tf_op jit(solution)/shard_map/dot_general | solution.py:129
  289.8 9.5 %reshape_reshape.10 = bf16[4,32,10,2048]{3,2,1,0:T(8,128)(2,1)} reshape(bf16[1280,2048]{1,0:T(8,128)(2,1)} %convolution_convert_fusion) | data formatting | bytes 10485760 | tf_op jit(solution)/shard_map/reshape;reshape | solution.py:24
  299.3 6.3 %copy.88 = bf16[4,32,10,2048]{3,1,2,0:T(8,128)(2,1)S(1)} copy(bf16[4,32,10,2048]{3,2,1,0:T(8,128)(2,1)} %reshape_reshape.10) | data formatting | bytes 10485760 | tf_op jit(solution)/shard_map/reshape;reshape | solution.py:24
  305.6 63.7 %all_to_all.46 = bf16[4,32,10,2048]{3,1,2,0:T(8,128)(2,1)} all-to-all(bf16[4,32,10,2048]{3,1,2,0:T(8,128)(2,1)S(1)} %copy.88), channel_id=1, replica_groups=mesh['grp'=2,'sp_0'=16,'sp_1'=2,'tp'=4] {'tp'}, dimensions={0} | all-to-all | bytes 10485760 | tf_op jit(solution)/shard_map/all_to_all | solution.py:29
  369.3 3.6 reduce_sum.72
  374.3 4.8 %all_to_all.47 = bf16[16,2,1,10,2048]{4,0,3,2,1:T(8,128)(2,1)S(1)} all-to-all(bf16[16,2,1,10,2048]{4,0,3,2,1:T(8,128)(2,1)S(1)} %copy.89), channel_id=1, replica_groups=mesh['grp'=2,'sp_0'=16,'sp_1'=2,'tp'=4] {'sp_1'}, dimensions={1} | all-to-all | bytes 2621440 | tf_op jit(solution)/shard_map/all_to_all | solution.py:43
  379.1 2.4 copy.90
  381.5 12.4 %all-to-all-start.5 = ((bf16[16,2,1,10,2048]{4,1,3,2,0:T(2,128)(2,1)}), bf16[16,2,1,10,2048]{4,1,3,2,0:T(2,128)(2,1)S(1)}, u32[]{:S(2)}, u32[]{:S(2)}) async-start(bf16[16,2,1,10,2048]{4,1,3,2,0:T(2,128)(2,1)} %copy.90), calls=%async_computation.5 | async-start | bytes 2621440 | tf_op jit(solution)/shard_map/all_to_all | solution.py:43
  394.4 60.1 %all-to-all-done.5 = bf16[16,2,1,10,2048]{4,1,3,2,0:T(2,128)(2,1)S(1)} async-done(((bf16[16,2,1,10,2048]{4,1,3,2,0:T(2,128)(2,1)}), bf16[16,2,1,10,2048]{4,1,3,2,0:T(2,128)(2,1)S(1)}, u32[]{:S(2)}, u32[]{:S(2)}) %all-to-all-start.5) | async-done | bytes 1310752 | tf_op jit(solution)/shard_map/all_to_all | solution.py:43
  454.6 2.0 copy.91
  456.6 2.5 reshape_reshape_reshape.7
  462.0 5.6 %multiply_reduce_fusion = f32[128,2048]{1,0:T(8,128)S(1)} fusion(bf16[128,2,2048]{2,1,0:T(2,128)(2,1)} %reshape.72, pred[128,2]{1,0:T(8,128)(4,1)S(1)} %copy.83, f32[128,2]{1,0:T(8,128)S(1)} %copy.78), kind=kLoop, calls=%fused_computation.10 | loop fusion | flops 1835008 | bytes 2098432 | tf_op jit(solution)/shard_map/reduce_sum | solution.py:138
  467.6 1.6 fusion.15
  (86 shorter events, 18.3 us)
Async XLA Ops:
  6.5 276.9 %copy-start = (bf16[1,768,2048]{2,1,0:T(8,128)(2,1)S(1)}, bf16[1,768,2048]{2,1,0:T(8,128)(2,1)}, u32[]{:S(2)}) copy-start(bf16[1,768,2048]{2,1,0:T(8,128)(2,1)} %param.29) | copy-start | bytes 9437188
  6.6 12.3 %copy-start.14 = (s32[512]{0:T(512)S(1)}, s32[512]{0:T(512)}, u32[]{:S(2)}) copy-start(s32[512]{0:T(512)} %param.19) | copy-start | bytes 6148
  6.6 10.6 %copy-start.15 = (s32[128,2]{0,1:T(2,128)S(1)}, s32[128,2]{0,1:T(2,128)}, u32[]{:S(2)}) copy-start(s32[128,2]{0,1:T(2,128)} %param.25) | copy-start | bytes 3076
  6.6 11.0 %copy-start.16 = (bf16[3,384]{1,0:T(4,128)(2,1)S(1)}, bf16[3,384]{1,0:T(4,128)(2,1)}, u32[]{:S(2)}) copy-start(bf16[3,384]{1,0:T(4,128)(2,1)} %param.20) | copy-start | bytes 6916
  6.6 87.6 %all-gather.3.cloned.1.call-start = ((), (), s32[]{:S(2)}) async-start(), calls=%async_computation.6 | async-start | bytes 7864320 | tf_op jit(solution)/shard_map/all_gather | solution.py:99
  8.3 10.5 %collective-permute-start = (f32[2]{0:T(128)S(1)}, f32[2]{0:T(128)S(1)}, u32[]{:S(2)}, u32[]{:S(2)}) collective-permute-start(f32[2]{0:T(128)S(1)} %slice.34), channel_id=1, source_target_pairs={{0,4},{4,8},{8,12},{12,16},{16,20},{20,24},{24,28},{28,32},{32,36}... | collective-permute-start | bytes 32 | tf_op jit(solution)/shard_map/ppermute | solution.py:19
  11.3 0.9 copy-start.5
  12.2 6.7 %collective-permute-start.1 = (f32[2,384]{1,0:T(2,128)S(1)}, f32[2,384]{1,0:T(2,128)S(1)}, u32[]{:S(2)}, u32[]{:S(2)}) collective-permute-start(f32[2,384]{1,0:T(2,128)S(1)} %slice.47), channel_id=1, source_target_pairs={{0,4},{4,8},{8,12},{12,16},{16,20},{20,24},{24,28},{28,32},{32,36}... | collective-permute-start | bytes 9224 | tf_op jit(solution)/shard_map/ppermute | solution.py:19
  22.0 12.8 %all-to-all-start = ((bf16[4,128,384]{2,1,0:T(8,128)(2,1)}), bf16[4,128,384]{2,1,0:T(8,128)(2,1)S(1)}, u32[]{:S(2)}, u32[]{:S(2)}) async-start(bf16[4,128,384]{2,1,0:T(8,128)(2,1)} %bitcast.46), calls=%async_computation | async-start | bytes 786432 | tf_op jit(solution)/shard_map/all_to_all | solution.py:95
  26.5 226.0 %all-gather.5.cloned.1.call-start = ((), (), s32[]{:S(2)}) async-start(), calls=%async_computation.7 | async-start | bytes 6553600 | tf_op jit(solution)/shard_map/all_gather | solution.py:120
  27.1 0.6 copy-start.10
  34.8 0.7 copy-start.6
  94.2 4.9 %copy-start.7 = (pred[320,128]{1,0:T(8,128)(4,1)S(1)}, pred[320,128]{1,0:T(8,128)(4,1)}, u32[]{:S(2)}) copy-start(pred[320,128]{1,0:T(8,128)(4,1)} %fusion.14) | copy-start | bytes 122884
  94.2 4.9 %copy-start.8 = (f32[2048]{0:T(1024)S(1)}, f32[2048]{0:T(1024)}, u32[]{:S(2)}) copy-start(f32[2048]{0:T(1024)} %param.24) | copy-start | bytes 24580
  94.2 4.9 %copy-start.9 = (f32[2048]{0:T(1024)S(1)}, f32[2048]{0:T(1024)}, u32[]{:S(2)}) copy-start(f32[2048]{0:T(1024)} %param.23) | copy-start | bytes 24580
  98.1 1.0 copy-start.2
  271.4 7.3 %copy-start.4 = (bf16[1280,2048]{1,0:T(8,128)(2,1)S(1)}, bf16[1280,2048]{1,0:T(8,128)(2,1)}, u32[]{:S(2)}) copy-start(bf16[1280,2048]{1,0:T(8,128)(2,1)} %reshape.70) | copy-start | bytes 15728644
  271.4 7.3 %copy-start.19 = (bf16[1,2048,768]{2,1,0:T(8,128)(2,1)S(1)}, bf16[1,2048,768]{2,1,0:T(8,128)(2,1)}, u32[]{:S(2)}) copy-start(bf16[1,2048,768]{2,1,0:T(8,128)(2,1)} %param.28) | copy-start | bytes 9437188
  379.1 14.8 %copy-start.11 = (s32[128,2]{0,1:T(2,128)S(1)}, s32[128,2]{0,1:T(2,128)}, u32[]{:S(2)}) copy-start(s32[128,2]{0,1:T(2,128)} %copy-done.10) | copy-start | bytes 3076
  379.1 15.1 %copy-start.17 = (pred[128,2]{0,1:T(4,128)(4,1)S(1)}, pred[128,2]{0,1:T(4,128)(4,1)}, u32[]{:S(2)}) copy-start(pred[128,2]{0,1:T(4,128)(4,1)} %get-tuple-element.8) | copy-start | bytes 772
  379.1 15.2 %copy-start.18 = (f32[128,2]{0,1:T(2,128)S(1)}, f32[128,2]{0,1:T(2,128)}, u32[]{:S(2)}) copy-start(f32[128,2]{0,1:T(2,128)} %param.26) | copy-start | bytes 3076
  381.5 73.1 %all-to-all-start.5 = ((bf16[16,2,1,10,2048]{4,1,3,2,0:T(2,128)(2,1)}), bf16[16,2,1,10,2048]{4,1,3,2,0:T(2,128)(2,1)S(1)}, u32[]{:S(2)}, u32[]{:S(2)}) async-start(bf16[16,2,1,10,2048]{4,1,3,2,0:T(2,128)(2,1)} %copy.90), calls=%async_computation.5 | async-start | bytes 2621440 | tf_op jit(solution)/shard_map/all_to_all | solution.py:43
  462.0 7.3 %copy-start.3 = (f32[128,2048]{1,0:T(8,128)S(1)}, f32[128,2048]{1,0:T(8,128)}, u32[]{:S(2)}) copy-start(f32[128,2048]{1,0:T(8,128)} %copy-done.2) | copy-start | bytes 3145732
  462.0 7.8 %copy-start.12 = (f32[2048]{0:T(1024)S(1)}, f32[2048]{0:T(1024)}, u32[]{:S(2)}) copy-start(f32[2048]{0:T(1024)} %param.31) | copy-start | bytes 24580
  462.0 7.8 %copy-start.13 = (f32[2048]{0:T(1024)S(1)}, f32[2048]{0:T(1024)}, u32[]{:S(2)}) copy-start(f32[2048]{0:T(1024)} %param.30) | copy-start | bytes 24580
  462.0 9.2 %copy-start.1 = (bf16[1,768,2048]{2,1,0:T(8,128)(2,1)S(1)}, bf16[1,768,2048]{2,1,0:T(8,128)(2,1)}, u32[]{:S(2)}) copy-start(bf16[1,768,2048]{2,1,0:T(8,128)(2,1)} %param.29) | copy-start | bytes 9437188
Sparse Core Ops, SparseCore 0:
  9.2 84.9 all-gather.2
  196.6 55.9 all-gather.4
where the time goes:
time: 479 us; the launch traced here: 478 us
  waiting for transfers between devices  181 us (38%)
  blocking collectives  151 us (32%)
  local copies, waits for them, and re-layouts  64.7 us (14%)
  matrix products  23.9 us (5%)
  starting transfers between devices  23.8 us (5%)
  other arithmetic  20.2 us (4%)
  between operations  13.7 us (3%)
    all_to_all x3, blocking collectives, moved_by_axis(): lax.all_to_all(tiles, axes[k], split_axis=k, concat_axis=k, tiled=True)  87.1 us
    all_to_all x1, blocking collectives, summed_on_arrival(): tiles = lax.all_to_all(split_up(x, dim, length), axis, 0, 0, tiled=True)  63.7 us
    all_to_all x1, waiting for transfers between devices, moved_by_axis(): lax.all_to_all(tiles, axes[k], split_axis=k, concat_axis=k, tiled=True)  60.1 us
    all_gather x1, waiting for transfers between devices, shards(): lax.all_gather(out_proj, 'tp', axis=0, tiled=True)  57.4 us
    all_gather x1, waiting for transfers between devices, shards(): lax.all_gather(two_step_exchange(packed, ('sp_0', 'sp_1'), (1, 0), 0, 0),...  56.1 us
    another operation x2, local copies, waits for them, and re-layouts, split_up(): return jnp.moveaxis(x.reshape(*before, length, -1, *after), dim, 0)  15.8 us
    all_to_all x1, starting transfers between devices, moved_by_axis(): lax.all_to_all(tiles, axes[k], split_axis=k, concat_axis=k, tiled=True)  12.4 us
    reshape x1, local copies, waits for them, and re-layouts, shards(): rows_in = whole.reshape(-1, shape_in[-1])  9.84 us
  transfers between devices with their start and end apart: 6, of which 4 were waited for; matrix products, arithmetic and copies ran while one was open for 2% of the time, Pallas kernels for 0%

commit v1 on v0

v1 whole, which is shorter than its diff:
```python
import jax
import jax.numpy as jnp
from jax import lax
from jax.sharding import Mesh
from jax.sharding import PartitionSpec as P

SP = ("sp_0", "sp_1")
GRP_SP = ("grp", "sp_0", "sp_1")
GRP_SP_TP = ("grp", "sp_0", "sp_1", "tp")
SUBLANES = 8

residual_scale = 2.0**0.5
norm_eps = 1e-05


def next_in_sequence(x):
    length = lax.axis_size(SP)
    return lax.ppermute(x, SP, [(i, i + 1) for i in range(length - 1)])


def swapped(x):
    return lax.ppermute(x, "sp_1", [(0, 1), (1, 0)])


def layer_norm(pre, gain, bias):
    center = pre - jnp.mean(pre, axis=-1, keepdims=True)
    spread = jnp.mean(center * center, axis=-1, keepdims=True)
    return center * lax.rsqrt(spread + norm_eps) * gain + bias


def dot(a, b):
    return jnp.dot(a, b, preferred_element_type=jnp.float32)


def chunk_slots(capacity, cores):
    width = SUBLANES // cores
    rest = capacity % width
    sizes = ([rest] if rest else []) + [width] * (capacity // width)
    starts = [sum(sizes[:i]) for i in range(len(sizes))]
    return list(zip(starts, sizes))


def shards(
    gate_in,
    mult_in,
    value_in,
    doc_ids,
    conv_taps,
    out_proj,
    resid,
    norm1_gain,
    norm1_bias,
    expert_ids,
    expert_wts,
    w_gate,
    w_up,
    w_down,
    norm2_gain,
    norm2_bias,
):
    n_tp = lax.axis_size("tp")
    chips = lax.axis_size("sp_0")
    cores = lax.axis_size("sp_1")
    experts = chips * cores
    tok_count, top_count = expert_ids.shape
    width = out_proj.shape[1]
    capacity = 5 * tok_count * top_count // (4 * experts)

    tap_weights = conv_taps.astype(jnp.float32)
    taps = tap_weights.shape[0]
    product = mult_in.astype(jnp.float32) * value_in.astype(jnp.float32)
    docs = doc_ids.astype(jnp.float32)
    row_count, channels = product.shape
    tail_docs = jnp.broadcast_to(docs[row_count - taps + 1 :, None], (taps - 1, channels))
    prev = next_in_sequence(jnp.concatenate([product[row_count - taps + 1 :], tail_docs], axis=0))
    prev_rows, prev_docs = prev[: taps - 1], prev[taps - 1 :, 0]
    meta = jnp.concatenate([expert_ids.astype(jnp.float32).T, expert_wts.T], axis=0)
    metas = jnp.stack([meta, swapped(meta)])

    ext_rows = jnp.concatenate([prev_rows, product], axis=0)
    ext_docs = jnp.concatenate([prev_docs, docs], axis=0)
    filtered = jnp.zeros_like(product)
    for tap_index in range(taps):
        shifted = ext_rows[tap_index : tap_index + row_count]
        same_doc = (ext_docs[tap_index : tap_index + row_count] == docs)[:, None]
        filtered = filtered + tap_weights[tap_index] * jnp.where(same_doc, shifted, 0.0)
    mixed_heads = (gate_in.astype(jnp.float32) * filtered).astype(jnp.bfloat16)
    partial = dot(mixed_heads, out_proj).astype(jnp.bfloat16)
    partials = lax.all_to_all(
        partial.reshape(n_tp, row_count // n_tp, width), "tp", 0, 0, tiled=True
    )
    mixed = jnp.sum(partials.astype(jnp.float32), axis=0)
    hidden_one = layer_norm(
        residual_scale * resid.astype(jnp.float32) + mixed, norm1_gain, norm1_bias
    ).astype(jnp.bfloat16)
    hidden_both = jnp.concatenate([hidden_one, swapped(hidden_one)], axis=0)

    ids, wts = metas[:, :top_count], metas[:, top_count:]
    numbers = (jnp.arange(chips) * cores + lax.axis_index("sp_1")).astype(jnp.float32)
    named = ids[:, :, None, :] == numbers[None, None, :, None]
    chosen = jnp.any(named, axis=1)
    weight = jnp.sum(jnp.where(named, wts[:, :, None, :], 0.0), axis=1)
    before = (jnp.arange(tok_count)[:, None] < jnp.arange(tok_count)[None, :]).astype(jnp.bfloat16)
    earlier = dot(chosen.astype(jnp.bfloat16), before)
    slot_of = jnp.where(chosen, earlier, -1.0)

    def selected(start, size, values):
        slots = (start + jnp.arange(size)).astype(jnp.float32)
        hit = slot_of.transpose(1, 0, 2)[:, :, None, None, :] == slots[None, None, :, None, None]
        same = jnp.arange(cores)[:, None] == jnp.arange(cores)[None, :]
        hit = hit & same[None, :, None, :, None]
        picked = jnp.where(hit, values.transpose(1, 0, 2)[:, :, None, None, :], 0.0)
        return picked.reshape(chips * cores * size, cores * tok_count)

    chunks = chunk_slots(capacity, cores)
    ones = jnp.ones_like(weight)
    packed = [
        dot(selected(start, size, ones).astype(jnp.bfloat16), hidden_both)
        .astype(jnp.bfloat16)
        .reshape(chips, cores * size, width)
        for start, size in chunks
    ]

    gathered = []
    for i in range(len(chunks)):
        moved = lax.all_to_all(packed[i], "sp_0", 0, 0, tiled=True)
        rest = tuple(packed[i + 1 :])
        moved, rest = lax.optimization_barrier((moved, rest))
        packed[i + 1 :] = list(rest)
        gathered.append(lax.all_gather(moved.reshape(-1, width), "tp", axis=0, tiled=True))
    scattered = []
    for rows_in in gathered:
        gate_act = dot(rows_in, w_gate[0])
        up_act = dot(rows_in, w_up[0])
        hid = (jax.nn.silu(gate_act) * up_act).astype(jnp.bfloat16)
        piece = dot(hid, w_down[0]).astype(jnp.bfloat16)
        scattered.append(lax.psum_scatter(piece, "tp", scatter_dimension=0, tiled=True))
    total = jnp.zeros((cores * tok_count, width), jnp.float32)
    for i, (start, size) in enumerate(chunks):
        ready = scattered[i].reshape(chips, cores * size, width)
        back = lax.all_to_all(ready, "sp_0", 0, 0, tiled=True).reshape(-1, width)
        factor = selected(start, size, weight)
        high = factor.astype(jnp.bfloat16)
        low = (factor - high.astype(jnp.float32)).astype(jnp.bfloat16)
        total = total + dot(high.T, back) + dot(low.T, back)
    moe = total[:tok_count] + swapped(total[tok_count:])
    return layer_norm(
        residual_scale * hidden_one.astype(jnp.float32) + moe, norm2_gain, norm2_bias
    ).astype(jnp.bfloat16)


def solution(mesh):
    torus = Mesh(
        mesh.devices.reshape(mesh.shape["grp"], -1, 2, mesh.shape["tp"]),
        ("grp", "sp_0", "sp_1", "tp"),
    )
    in_specs = (
        P(GRP_SP, "tp"),
        P(GRP_SP, "tp"),
        P(GRP_SP, "tp"),
        P(GRP_SP),
        P(None, "tp"),
        P("tp", None),
        P(GRP_SP_TP, None),
        P(),
        P(),
        P(GRP_SP_TP, None),
        P(GRP_SP_TP, None),
        P(SP, None, "tp"),
        P(SP, None, "tp"),
        P(SP, "tp", None),
        P(),
        P(),
    )
    out_specs = P(GRP_SP_TP, None)
    return jax.shard_map(
        shards, mesh=torus, in_specs=in_specs, out_specs=out_specs, check_vma=False
    )
```

time: 479 us -> 385 us (0.80)
  local copies, waits for them, and re-layouts: 64.7 us -> 5.08 us
  waiting for transfers between devices: 181 us -> 135 us
  blocking collectives: 151 us -> 106 us
  matrix products: 23.9 us -> 57.2 us
  starting transfers between devices: 23.8 us -> 52.5 us
  other arithmetic: 20.2 us -> 11.9 us
    all_gather x2 -> x3, waiting for transfers between devices: 114 us -> 21.1 us  [shards(): lax.all_gather(moved.reshape(-1, width), 'tp', axis=0, tiled=True)]
    all_to_all x4 -> x3, blocking collectives: 151 us -> 106 us  [the longest x2 70.7 us: shards(): back = lax.all_to_all(ready, 'sp_0', 0, 0, tiled=True).reshape(-1, width)]
    dot_general x5 -> x17, matrix products: 23.9 us -> 57.2 us  [dot(): return jnp.dot(a, b, preferred_element_type=jnp.float32)]
    another operation x9 -> x0, local copies, waits for them, and re-layouts: 29.5 us -> none  [the longest x2 15.8 us: split_up(): return jnp.moveaxis(x.reshape(*before, length, -1, *after), dim, 0)]
    all_to_all x2 -> x4, starting transfers between devices: 17 us -> 45.1 us  [the longest x2 31.3 us: shards(): moved = lax.all_to_all(packed[i], 'sp_0', 0, 0, tiled=True)]
    reduce_scatter x0 -> x3, waiting for transfers between devices: none -> 26 us  [shards(): lax.psum_scatter(piece, 'tp', scatter_dimension=0, tiled=True)]
    all_to_all x2 -> x4, waiting for transfers between devices: 66.6 us -> 83.7 us  [the longest x2 40.9 us: shards(): moved = lax.all_to_all(packed[i], 'sp_0', 0, 0, tiled=True)]
    all_to_all x5 -> x0, local copies, waits for them, and re-layouts: 9.15 us -> none  [the longest x4 7.93 us: moved_by_axis(): lax.all_to_all(tiles, axes[k], split_axis=k, concat_axis=k, tiled=True)]
  transfers between devices with their start and end apart: 6 -> 14, of which waited for: 4 -> 11; matrix products, arithmetic and copies ran while one was open for 2% -> 14% of each run, Pallas kernels for 0% -> 0%
where the time goes in v1:
time: 385 us; the launch traced here: 382 us
  waiting for transfers between devices  135 us (35%)
  blocking collectives  106 us (28%)
  matrix products  57.2 us (15%)
  starting transfers between devices  52.5 us (14%)
  between operations  13.9 us (4%)
  other arithmetic  11.9 us (3%)
  local copies, waits for them, and re-layouts  5.08 us (1%)
    all_to_all x2, blocking collectives, shards(): back = lax.all_to_all(ready, 'sp_0', 0, 0, tiled=True).reshape(-1, width)  70.7 us
    dot_general x17, matrix products, dot(): return jnp.dot(a, b, preferred_element_type=jnp.float32)  57.2 us
    all_to_all x2, waiting for transfers between devices, shards(): moved = lax.all_to_all(packed[i], 'sp_0', 0, 0, tiled=True)  40.9 us
    all_to_all x1, blocking collectives, shards(): moved = lax.all_to_all(packed[i], 'sp_0', 0, 0, tiled=True)  35.6 us
    all_to_all x2, starting transfers between devices, shards(): moved = lax.all_to_all(packed[i], 'sp_0', 0, 0, tiled=True)  31.3 us
    reduce_scatter x3, waiting for transfers between devices, shards(): lax.psum_scatter(piece, 'tp', scatter_dimension=0, tiled=True)  26 us
    all_to_all x1, waiting for transfers between devices, shards(): lax.all_to_all(partial.reshape(n_tp, row_count // n_tp, width), 'tp', 0,...  21.9 us
    all_gather x3, waiting for transfers between devices, shards(): lax.all_gather(moved.reshape(-1, width), 'tp', axis=0, tiled=True)  21.1 us
  transfers between devices with their start and end apart: 14, of which 11 were waited for; matrix products, arithmetic and copies ran while one was open for 14% of the time, Pallas kernels for 0%

profile of v1, /device:TPU:40, one launch (start us, length us, event | category | flops | bytes accessed | tf_op | source)
XLA Modules:
  0.0 382.1 jit_solution(6780999300419874182)
XLA Ops:
  8.9 1.8 collective-permute-start
  12.5 4.4 %convolution_convert_fusion = bf16[512,2048]{1,0:T(8,128)(2,1)} fusion(bf16[384,2048]{1,0:T(8,128)(2,1)} %param.21, f32[2,384]{1,0:T(2,128)S(1)} %slice.63, f32[512,384]{1,0:T(8,128)S(1)} %convert_multiply_fusion, bf16[512,384]{1,0:T(8,128)(2,1)} %param.16, f32[384]{0:T(512)S(1)} %get-tuple-element.16, f32[384]{0:T(512)S(1)} %get-tuple-element.17, ...), kind=kOutput, calls=%fused_computation.21 | convolution fusion | flops 808910848 | bytes 4858880 | tf_op jit(solution)/shard_map/dot_general | solution.py:32
  16.9 4.7 %all-to-all-start = ((bf16[4,128,2048]{2,1,0:T(8,128)(2,1)}), bf16[4,128,2048]{2,1,0:T(8,128)(2,1)}, u32[]{:S(2)}, u32[]{:S(2)}) async-start(bf16[4,128,2048]{2,1,0:T(8,128)(2,1)} %bitcast.127), calls=%async_computation | async-start | bytes 4194304 | tf_op jit(solution)/shard_map/all_to_all | solution.py:89
  21.6 3.0 collective-permute-start.1
  25.7 21.9 %all-to-all-done = bf16[4,128,2048]{2,1,0:T(8,128)(2,1)} async-done(((bf16[4,128,2048]{2,1,0:T(8,128)(2,1)}), bf16[4,128,2048]{2,1,0:T(8,128)(2,1)}, u32[]{:S(2)}, u32[]{:S(2)}) %all-to-all-start) | async-done | bytes 2097184 | tf_op jit(solution)/shard_map/all_to_all | solution.py:89
  47.6 2.1 convert_reduce_fusion
  50.7 1.8 collective-permute-start.2
  56.0 25.1 %all-to-all-start.1 = ((bf16[16,4,2048]{2,1,0:T(4,128)(2,1)}), bf16[16,4,2048]{2,1,0:T(4,128)(2,1)S(1)}, u32[]{:S(2)}, u32[]{:S(2)}) async-start(bf16[16,4,2048]{2,1,0:T(4,128)(2,1)} %reshape.246), calls=%async_computation.1 | async-start | bytes 524288 | tf_op jit(solution)/shard_map/all_to_all | solution.py:126
  81.3 1.8 fusion.83
  83.0 2.3 fusion.31
  86.5 12.9 %all-to-all-done.1 = bf16[16,4,2048]{2,1,0:T(4,128)(2,1)S(1)} async-done(((bf16[16,4,2048]{2,1,0:T(4,128)(2,1)}), bf16[16,4,2048]{2,1,0:T(4,128)(2,1)S(1)}, u32[]{:S(2)}, u32[]{:S(2)}) %all-to-all-start.1) | async-done | bytes 262176 | tf_op jit(solution)/shard_map/all_to_all | solution.py:126
  99.4 6.2 %all-to-all-start.3 = ((bf16[16,8,2048]{2,1,0:T(8,128)(2,1)}), bf16[16,8,2048]{2,1,0:T(8,128)(2,1)}, u32[]{:S(2)}, u32[]{:S(2)}) async-start(bf16[16,8,2048]{2,1,0:T(8,128)(2,1)} %fusion.31), calls=%async_computation.4 | async-start | bytes 1048576 | tf_op jit(solution)/shard_map/all_to_all | solution.py:126
  106.6 28.0 %all-to-all-done.3 = bf16[16,8,2048]{2,1,0:T(8,128)(2,1)} async-done(((bf16[16,8,2048]{2,1,0:T(8,128)(2,1)}), bf16[16,8,2048]{2,1,0:T(8,128)(2,1)}, u32[]{:S(2)}, u32[]{:S(2)}) %all-to-all-start.3) | async-done | bytes 524320 | tf_op jit(solution)/shard_map/all_to_all | solution.py:126
  134.7 35.6 %all_to_all.35 = bf16[16,8,2048]{2,1,0:T(8,128)(2,1)} all-to-all(bf16[16,8,2048]{2,1,0:T(8,128)(2,1)} %fusion.32), channel_id=1, replica_groups=mesh['grp'=2,'sp_0'=16,'sp_1'=2,'tp'=4] {'sp_0'}, dimensions={0} | all-to-all | bytes 1048576 | tf_op jit(solution)/shard_map/all_to_all | solution.py:126
  170.5 4.1 %fusion.16 = f32[256,768]{1,0:T(8,128)} fusion(bf16[256,2048]{1,0:T(8,128)(2,1)} %all-gather.4.cloned.1.call-done, bf16[1,2048,768]{2,1,0:T(8,128)(2,1)} %param.27), kind=kOutput, calls=%fused_computation.17 | convolution fusion | flops 805306368 | bytes 4980736 | tf_op jit(solution)/shard_map/dot_general | solution.py:32
  174.6 5.6 %fusion.28 = bf16[256,2048]{1,0:T(8,128)(2,1)} fusion(bf16[1,768,2048]{2,1,0:T(8,128)(2,1)S(1)} %copy-done, bf16[256,2048]{1,0:T(8,128)(2,1)} %all-gather.4.cloned.1.call-done, bf16[1,2048,768]{2,1,0:T(8,128)(2,1)} %param.28, f32[256,768]{1,0:T(8,128)} %fusion.16), kind=kOutput, calls=%fused_computation.27 | convolution fusion | flops 1612316672 | bytes 9175040 | tf_op jit(solution)/shard_map/dot_general | solution.py:32
  180.5 5.5 %fusion.14 = f32[512,768]{1,0:T(8,128)} fusion(bf16[512,2048]{1,0:T(8,128)(2,1)} %all-gather.6.cloned.1.call-done, bf16[1,2048,768]{2,1,0:T(8,128)(2,1)} %param.27), kind=kOutput, calls=%fused_computation.15 | convolution fusion | flops 1610612736 | bytes 6815744 | tf_op jit(solution)/shard_map/dot_general | solution.py:32
  186.0 8.2 %fusion.18 = bf16[512,2048]{1,0:T(8,128)(2,1)} fusion(bf16[1,768,2048]{2,1,0:T(8,128)(2,1)S(1)} %copy-done, f32[512,768]{1,0:T(8,128)} %fusion.14, bf16[512,2048]{1,0:T(8,128)(2,1)} %all-gather.6.cloned.1.call-done, bf16[1,2048,768]{2,1,0:T(8,128)(2,1)} %param.28), kind=kOutput, calls=%fused_computation.19 | convolution fusion | flops 3224633344 | bytes 12058624 | tf_op jit(solution)/shard_map/dot_general | solution.py:32
  194.3 21.1 %all-gather.8.cloned.1.call-done = bf16[512,2048]{1,0:T(8,128)(2,1)} async-done(((bf16[128,2048]{1,0:T(8,128)(2,1)}), bf16[512,2048]{1,0:T(8,128)(2,1)}) %all-gather.8.cloned.1.call-update) | async-done | bytes 2097168 | tf_op jit(solution)/shard_map/all_gather | solution.py:130
  215.4 5.5 %fusion.12 = f32[512,768]{1,0:T(8,128)} fusion(bf16[512,2048]{1,0:T(8,128)(2,1)} %all-gather.8.cloned.1.call-done, bf16[1,2048,768]{2,1,0:T(8,128)(2,1)} %param.27), kind=kOutput, calls=%fused_computation.13 | convolution fusion | flops 1610612736 | bytes 6815744 | tf_op jit(solution)/shard_map/dot_general | solution.py:32
  220.9 8.3 %fusion.21 = bf16[512,2048]{1,0:T(8,128)(2,1)} fusion(bf16[1,768,2048]{2,1,0:T(8,128)(2,1)S(1)} %copy-done, f32[512,768]{1,0:T(8,128)} %fusion.12, bf16[512,2048]{1,0:T(8,128)(2,1)} %all-gather.8.cloned.1.call-done, bf16[1,2048,768]{2,1,0:T(8,128)(2,1)} %param.28), kind=kOutput, calls=%fused_computation.20 | convolution fusion | flops 3224633344 | bytes 12058624 | tf_op jit(solution)/shard_map/dot_general | solution.py:32
  229.3 18.5 %reduce-scatter.4.cloned.1.call-done = bf16[64,2048]{1,0:T(8,128)(2,1)} async-done(((bf16[256,2048]{1,0:T(8,128)(2,1)}), bf16[64,2048]{1,0:T(8,128)(2,1)}) %reduce-scatter.4.cloned.1.call-update) | async-done | bytes 262160 | tf_op jit(solution)/shard_map/reduce_scatter | solution.py:137
  248.8 29.4 %all_to_all.36 = bf16[16,4,2048]{2,1,0:T(4,128)(2,1)} all-to-all(bf16[16,4,2048]{2,1,0:T(4,128)(2,1)S(1)} %reshape.250), channel_id=1, replica_groups=mesh['grp'=2,'sp_0'=16,'sp_1'=2,'tp'=4] {'sp_0'}, dimensions={0} | all-to-all | bytes 524288 | tf_op jit(solution)/shard_map/all_to_all | solution.py:141
  278.2 7.5 %reduce-scatter.6.cloned.1.call-done = bf16[128,2048]{1,0:T(8,128)(2,1)} async-done(((bf16[512,2048]{1,0:T(8,128)(2,1)}), bf16[128,2048]{1,0:T(8,128)(2,1)}) %reduce-scatter.6.cloned.1.call-update) | async-done | bytes 524304 | tf_op jit(solution)/shard_map/reduce_scatter | solution.py:137
  285.7 41.3 %all_to_all.37 = bf16[16,8,2048]{2,1,0:T(8,128)(2,1)} all-to-all(bf16[16,8,2048]{2,1,0:T(8,128)(2,1)} %bitcast.130), channel_id=1, replica_groups=mesh['grp'=2,'sp_0'=16,'sp_1'=2,'tp'=4] {'sp_0'}, dimensions={0} | all-to-all | bytes 1048576 | tf_op jit(solution)/shard_map/all_to_all | solution.py:141
  327.0 9.1 %all-to-all-start.6 = ((bf16[16,8,2048]{2,1,0:T(8,128)(2,1)}), bf16[16,8,2048]{2,1,0:T(8,128)(2,1)}, u32[]{:S(2)}, u32[]{:S(2)}) async-start(bf16[16,8,2048]{2,1,0:T(8,128)(2,1)} %bitcast.129), calls=%async_computation.9 | async-start | bytes 1048576 | tf_op jit(solution)/shard_map/all_to_all | solution.py:141
  337.9 2.6 fusion.109
  340.5 1.8 fusion.64
  342.3 1.8 fusion.66
  344.1 20.9 %all-to-all-done.6 = bf16[16,8,2048]{2,1,0:T(8,128)(2,1)} async-done(((bf16[16,8,2048]{2,1,0:T(8,128)(2,1)}), bf16[16,8,2048]{2,1,0:T(8,128)(2,1)}, u32[]{:S(2)}, u32[]{:S(2)}) %all-to-all-start.6) | async-done | bytes 524320 | tf_op jit(solution)/shard_map/all_to_all | solution.py:141
  368.2 2.5 fusion.27
  371.0 2.6 collective-permute-done.3
  (112 shorter events, 20.2 us)
Async XLA Ops:
  6.5 168.1 %copy-start = (bf16[1,768,2048]{2,1,0:T(8,128)(2,1)S(1)}, bf16[1,768,2048]{2,1,0:T(8,128)(2,1)}, u32[]{:S(2)}) copy-start(bf16[1,768,2048]{2,1,0:T(8,128)(2,1)} %param.29) | copy-start | bytes 9437188
  8.9 2.6 collective-permute-start
  16.9 4.7 %copy-start.19 = (s32[128,2]{0,1:T(2,128)S(1)}, s32[128,2]{0,1:T(2,128)}, u32[]{:S(2)}) copy-start(s32[128,2]{0,1:T(2,128)} %param.25) | copy-start | bytes 3076
  16.9 4.7 %copy-start.20 = (f32[128,2]{0,1:T(2,128)S(1)}, f32[128,2]{0,1:T(2,128)}, u32[]{:S(2)}) copy-start(f32[128,2]{0,1:T(2,128)} %param.26) | copy-start | bytes 3076
  16.9 30.7 %all-to-all-start = ((bf16[4,128,2048]{2,1,0:T(8,128)(2,1)}), bf16[4,128,2048]{2,1,0:T(8,128)(2,1)}, u32[]{:S(2)}, u32[]{:S(2)}) async-start(bf16[4,128,2048]{2,1,0:T(8,128)(2,1)} %bitcast.127), calls=%async_computation | async-start | bytes 4194304 | tf_op jit(solution)/shard_map/all_to_all | solution.py:89
  21.6 3.9 %collective-permute-start.1 = (f32[4,128]{1,0:T(4,128)S(1)}, f32[4,128]{1,0:T(4,128)S(1)}, u32[]{:S(2)}, u32[]{:S(2)}) collective-permute-start(f32[4,128]{1,0:T(4,128)S(1)} %get-tuple-element.36), channel_id=1, source_target_pairs={{0,4},{4,0},{1,5},{5,1},{2,6},{6,2},{3,7},{7,3},{8,12},{12,8},{9,1... | collective-permute-start | bytes 6152 | tf_op jit(solution)/shard_map/ppermute | solution.py:22
  24.7 28.1 %copy-start.17 = (pred[2,2]{1,0:T(4,128)(4,1)}, pred[2,2]{1,0:T(4,128)(4,1)S(1)}, u32[]{:S(2)}) copy-start(pred[2,2]{1,0:T(4,128)(4,1)S(1)} %iota_compare_fusion.1) | copy-start | bytes 16
  50.7 3.4 copy-start.5
  50.7 3.4 collective-permute-start.2
  56.0 43.4 %all-to-all-start.1 = ((bf16[16,4,2048]{2,1,0:T(4,128)(2,1)}), bf16[16,4,2048]{2,1,0:T(4,128)(2,1)S(1)}, u32[]{:S(2)}, u32[]{:S(2)}) async-start(bf16[16,4,2048]{2,1,0:T(4,128)(2,1)} %reshape.246), calls=%async_computation.1 | async-start | bytes 524288 | tf_op jit(solution)/shard_map/all_to_all | solution.py:126
  81.1 4.3 %copy-start.6 = (bf16[128,2048]{1,0:T(8,128)(2,1)S(1)}, bf16[128,2048]{1,0:T(8,128)(2,1)}, u32[]{:S(2)}) copy-start(bf16[128,2048]{1,0:T(8,128)(2,1)} %copy-done.5) | copy-start | bytes 1572868
  81.1 4.2 %copy-start.22 = (bf16[128,2048]{1,0:T(8,128)(2,1)S(1)}, bf16[128,2048]{1,0:T(8,128)(2,1)}, u32[]{:S(2)}) copy-start(bf16[128,2048]{1,0:T(8,128)(2,1)} %copy-done.21) | copy-start | bytes 1572868
  99.4 35.2 %all-to-all-start.3 = ((bf16[16,8,2048]{2,1,0:T(8,128)(2,1)}), bf16[16,8,2048]{2,1,0:T(8,128)(2,1)}, u32[]{:S(2)}, u32[]{:S(2)}) async-start(bf16[16,8,2048]{2,1,0:T(8,128)(2,1)} %fusion.31), calls=%async_computation.4 | async-start | bytes 1048576 | tf_op jit(solution)/shard_map/all_to_all | solution.py:126
  105.6 64.9 %all-gather.4.cloned.1.call-start = ((), (), s32[]{:S(2)}) async-start(), calls=%async_computation.10 | async-start | bytes 1310720 | tf_op jit(solution)/shard_map/all_gather | solution.py:130
  106.5 74.0 %all-gather.6.cloned.1.call-start = ((), (), s32[]{:S(2)}) async-start(), calls=%async_computation.12 | async-start | bytes 2621440 | tf_op jit(solution)/shard_map/all_gather | solution.py:130
  134.7 80.8 %all-gather.8.cloned.1.call-start = ((), (), s32[]{:S(2)}) async-start(), calls=%async_computation.14 | async-start | bytes 2621440 | tf_op jit(solution)/shard_map/all_gather | solution.py:130
  170.4 77.3 %reduce-scatter.4.cloned.1.call-start = ((), (), s32[]{:S(2)}) async-start(), calls=%async_computation.11 | async-start | bytes 1310720 | tf_op jit(solution)/shard_map/reduce_scatter | solution.py:137
  180.2 105.5 %reduce-scatter.6.cloned.1.call-start = ((), (), s32[]{:S(2)}) async-start(), calls=%async_computation.13 | async-start | bytes 2621440 | tf_op jit(solution)/shard_map/reduce_scatter | solution.py:137
  194.3 132.8 %reduce-scatter.8.cloned.1.call-start = ((), (), s32[]{:S(2)}) async-start(), calls=%async_computation.15 | async-start | bytes 2621440 | tf_op jit(solution)/shard_map/reduce_scatter | solution.py:137
  278.2 58.0 %copy-start.11 = (pred[16,2,2,128]{3,2,1,0:T(4,128)(4,1)S(1)}, pred[16,2,2,128]{3,2,1,0:T(4,128)(4,1)}, u32[]{:S(2)}) copy-start(pred[16,2,2,128]{3,2,1,0:T(4,128)(4,1)} %copy-done.10) | copy-start | bytes 24580
  278.2 58.0 %copy-start.18 = (pred[2,2]{1,0:T(4,128)(4,1)S(1)}, pred[2,2]{1,0:T(4,128)(4,1)}, u32[]{:S(2)}) copy-start(pred[2,2]{1,0:T(4,128)(4,1)} %copy-done.17) | copy-start | bytes 16
  327.0 38.0 %all-to-all-start.6 = ((bf16[16,8,2048]{2,1,0:T(8,128)(2,1)}), bf16[16,8,2048]{2,1,0:T(8,128)(2,1)}, u32[]{:S(2)}, u32[]{:S(2)}) async-start(bf16[16,8,2048]{2,1,0:T(8,128)(2,1)} %bitcast.129), calls=%async_computation.9 | async-start | bytes 1048576 | tf_op jit(solution)/shard_map/all_to_all | solution.py:141
  337.9 2.6 copy-start.4
  337.9 2.6 copy-start.9
  337.9 4.4 %copy-start.8 = (bf16[16,2,4,2,128]{4,3,2,1,0:T(2,128)(2,1)S(1)}, bf16[16,2,4,2,128]{4,3,2,1,0:T(2,128)(2,1)}, u32[]{:S(2)}) copy-start(bf16[16,2,4,2,128]{4,3,2,1,0:T(2,128)(2,1)} %get-tuple-element.21) | copy-start | bytes 196612
  365.0 3.2 copy-start.1
  365.0 3.2 copy-start.2
  365.0 3.2 copy-start.12
  370.7 2.9 copy-start.7
  370.8 3.4 copy-start.15
  370.8 3.4 copy-start.16
  370.8 2.8 collective-permute-start.3
  (5 other events, 5.7 us)
Sparse Core Ops, SparseCore 0:
  108.3 29.2 all-gather.3
  139.4 37.2 all-gather.5
  178.5 36.8 all-gather.7
  217.9 29.7 reduce-scatter.3
  250.1 35.5 reduce-scatter.5
  288.1 35.5 reduce-scatter.7
